TPU v7x, 32 devices: a whole 2x2x4 slice. The times are simulated.
32 devices in a mesh: dp: 4 (over y, x), kv: 4 (over z), tp: 2 (over core).
Axes of the slice: x: 2, y: 2, z: 4, core: 2. Of those that a mesh axis runs over, the one named last changes fastest.
Arguments:
- tokens: bfloat16 [4, 16, 2048], P('dp', None, 'kv'), may hold values from -18 to 18, as said below
- norm_gain: float32 [2048], P('kv'), may hold values from 0.1 to 1.9
- w_query: bfloat16 [2048, 3072], P('kv', 'tp'), may hold values from -0.125 to 0.125
- w_key: bfloat16 [2048, 3072], P('kv', 'tp'), may hold values from -0.125 to 0.125
- w_value: bfloat16 [2048, 3072], P('kv', 'tp'), may hold values from -0.125 to 0.125
- w_gate: bfloat16 [2048, 3072], P('kv', 'tp'), may hold values from -0.125 to 0.125
- w_out: bfloat16 [3072, 2048], P('tp', 'kv'), may hold values from -0.109375 to 0.109375
- head_bias: float32 [24], P('tp'), may hold values from -14 to -2
- cache_keys: bfloat16 [4, 2048, 24, 128], P('dp', 'kv', 'tp'), may hold values from -18 to 18, as said below
- cache_values: bfloat16 [4, 2048, 24, 128], P('dp', 'kv', 'tp'), may hold values from -6 to 6
- prefix_len: int32 [4], P('dp'), may hold values from 1536 to 2028
- accepted: int32 [4], P('dp'), may hold values from 1 to 4
- parent: int32 [4, 16], P('dp'), may hold values from -1 to 14, as said below
Outputs:
- mixed: bfloat16 [4, 16, 2048], P('dp', None, 'kv')
- keys_next: bfloat16 [4, 2048, 24, 128], P('dp', 'kv', 'tp')
- values_next: bfloat16 [4, 2048, 24, 128], P('dp', 'kv', 'tp')
Inputs may be any that keep to these rules, and one draw needn't show every extreme that they name: `tokens`: entries of order one. `cache_keys`: entries of order one. parent of proposal 0 is -1; for p of 1 or more, parent[p] lies in max(p - 3, 0) to p - 1.
All inputs are finite; a program needn't handle non-finite values.
Results may differ from a plain program's by a relative error of at most 0.012.
Values may be sent and summed in bfloat16 or wider, within the bound.
A program may use at most 64 MiB of HBM per device.

v0:
```python
import jax
import jax.numpy as jnp
from jax import lax
from jax.sharding import PartitionSpec as P

D = 2048
HEAD = 128
EPS = 1e-06


def ancestry(parent):
    count = parent.shape[-1]
    places = jnp.arange(count, dtype=jnp.int32)
    reach = (parent[:, :, None] == places[None, None, :]).astype(jnp.float32)
    for repeat in range(count.bit_length()):
        reach = jnp.minimum(
            reach + jnp.einsum("spj,sjk->spk", reach, reach, precision=lax.Precision.HIGHEST), 1.0
        )
    return reach > 0.5


def after_table(count):
    places = jnp.arange(count, dtype=jnp.int32)
    return (places[:, None] > places[None, :]).astype(jnp.float32)


def sum_after(values):
    table = after_table(values.shape[-1])
    return jnp.einsum("shpk,kc->shpc", values, table, precision=lax.Precision.HIGHEST)


def local(
    tokens,
    norm_gain,
    w_query,
    w_key,
    w_value,
    w_gate,
    w_out,
    head_bias,
    cache_keys,
    cache_values,
    prefix_len,
    accepted,
    parent,
):
    seqs, props, columns = tokens.shape
    width = w_query.shape[1]
    heads = width // HEAD
    flat = tokens.astype(jnp.float32).reshape(seqs * props, columns)
    square_part = jnp.sum(flat * flat, axis=1)
    scaled = (flat * norm_gain).astype(jnp.bfloat16)
    partial_value = jnp.concatenate(
        [
            jnp.dot(scaled, weight, preferred_element_type=jnp.float32)
            for weight in (w_query, w_key, w_value, w_gate)
        ],
        axis=1,
    )
    squares = lax.psum(square_part, "kv")
    share = lax.psum_scatter(partial_value, "kv", scatter_dimension=1, tiled=True)
    rscale = lax.rsqrt(squares / D + EPS)
    projected = lax.all_gather(
        (share * rscale[:, None]).astype(jnp.bfloat16), "kv", axis=1, tiled=True
    )
    shaped = projected.reshape(seqs, props, 4, heads, HEAD)
    query = shaped[:, :, 0]
    key_new = shaped[:, :, 1]
    value_new = shaped[:, :, 2]
    gate = projected[:, 3 * width :].astype(jnp.float32)
    factor = HEAD ** (-0.5)
    bias_col = head_bias[None, :, None, None]
    ctx_dev = cache_keys.shape[1]
    places = lax.axis_index("kv") * ctx_dev + jnp.arange(ctx_dev, dtype=jnp.int32)
    valid = prefix_len + accepted
    live = (places[None, :] < valid[:, None])[:, None, None, :]
    scores = (
        jnp.einsum("sphd,schd->shpc", query, cache_keys, preferred_element_type=jnp.float32)
        * factor
        + bias_col
    )
    keep_log = jnp.where(live, jax.nn.log_sigmoid(-scores), 0.0)
    shard_rest = jnp.sum(keep_log, axis=3)
    family = ancestry(parent)[:, None]
    tree_scores = (
        jnp.einsum("sphd,sjhd->shpj", query, key_new, preferred_element_type=jnp.float32) * factor
        + bias_col
    )
    tree_keep = jnp.where(family, jax.nn.log_sigmoid(-tree_scores), 0.0)
    tail = jnp.sum(tree_keep, axis=3)
    every = lax.all_gather(shard_rest[None], "kv", axis=0, tiled=True)
    after = jnp.arange(every.shape[0], dtype=jnp.int32) > lax.axis_index("kv")
    beyond = jnp.sum(jnp.where(after[:, None, None, None], every, 0.0), axis=0)
    later_cache = sum_after(keep_log) + (beyond + tail)[..., None]
    cache_weight = jnp.where(live, jnp.exp(jax.nn.log_sigmoid(scores) + later_cache), 0.0).astype(
        jnp.bfloat16
    )
    later_tree = sum_after(tree_keep)
    tree_weight = jnp.where(
        family, jnp.exp(jax.nn.log_sigmoid(tree_scores) + later_tree), 0.0
    ).astype(jnp.bfloat16)
    local_sum = jnp.einsum(
        "shpc,schd->sphd", cache_weight, cache_values, preferred_element_type=jnp.float32
    )
    attended = lax.psum(local_sum, "kv")
    attended = attended + jnp.einsum(
        "shpj,sjhd->sphd", tree_weight, value_new, preferred_element_type=jnp.float32
    )
    mixin = (attended.reshape(seqs * props, width) * jax.nn.silu(gate)).astype(jnp.bfloat16)
    part_out = jnp.dot(mixin, w_out, preferred_element_type=jnp.float32).astype(jnp.bfloat16)
    part_out = lax.optimization_barrier(part_out).astype(jnp.float32)
    mixed = lax.psum(part_out.astype(jnp.bfloat16), "tp").reshape(seqs, props, w_out.shape[1])
    relative = places[None, :] - valid[:, None]
    picker = (relative[:, :, None] == jnp.arange(props, dtype=jnp.int32)[None, None, :]).astype(
        jnp.bfloat16
    )
    inside = ((relative >= 0) & (relative < props))[:, :, None, None]
    placed_keys = jnp.einsum(
        "scp,sphd->schd", picker, key_new, preferred_element_type=jnp.float32
    ).astype(jnp.bfloat16)
    placed_values = jnp.einsum(
        "scp,sphd->schd", picker, value_new, preferred_element_type=jnp.float32
    ).astype(jnp.bfloat16)
    keys_next = jnp.where(inside, placed_keys, cache_keys)
    values_next = jnp.where(inside, placed_values, cache_values)
    return (mixed, keys_next, values_next)


def solution(mesh):
    return jax.shard_map(
        local,
        mesh=mesh,
        in_specs=(
            P("dp", None, "kv"),
            P("kv"),
            P("kv", "tp"),
            P("kv", "tp"),
            P("kv", "tp"),
            P("kv", "tp"),
            P("tp", "kv"),
            P("tp"),
            P("dp", "kv", "tp", None),
            P("dp", "kv", "tp", None),
            P("dp"),
            P("dp"),
            P("dp", None),
        ),
        out_specs=(P("dp", None, "kv"), P("dp", "kv", "tp", None), P("dp", "kv", "tp", None)),
        check_vma=False,
    )
```

profile of v0, /device:TPU:0, one launch (start us, length us, event | category | flops | bytes accessed | tf_op | source)
XLA Modules:
  0.0 114.4 jit_solution(16729290940814623827)
XLA Ops:
  7.3 1.3 %copy-done = bf16[512,1536]{1,0:T(8,128)(2,1)S(1)} copy-done((bf16[512,1536]{1,0:T(8,128)(2,1)S(1)}, bf16[512,1536]{1,0:T(8,128)(2,1)}, u32[]{:S(2)}) %copy-start) | copy-done | bytes 1572888
  8.6 1.1 fusion.70
  9.8 0.3 fusion.68
  10.1 0.3 fusion.66
  10.4 0.8 copy-done.6
  11.3 0.3 fusion.64
  11.6 0.8 pad_maximum_fusion
  12.4 0.2 fusion.26
  12.6 0.1 fusion.22
  12.8 0.1 fusion.23
  12.9 0.1 fusion.24
  13.0 0.2 fusion.27
  14.7 13.6 %psum.21 = f32[16]{0:T(128)S(1)} all-reduce(f32[16]{0:T(128)S(1)} %fusion.52), channel_id=1, replica_groups=mesh['dp'=4,'kv'=4,'tp'=2] {'kv'}, use_global_device_ids=true, to_apply=%region_2.0 | all-reduce | flops 16 | bytes 128 | tf_op jit(solution)/shard_map/psum | solution.py:60
  28.4 7.6 %reduce-scatter.2.cloned.1.call-done = f32[16,1536]{1,0:T(8,128)} async-done(((f32[16,6144]{1,0:T(8,128)}), f32[16,1536]{1,0:T(8,128)}) %reduce-scatter.2.cloned.1.call-update) | async-done | bytes 98320 | tf_op jit(solution)/shard_map/reduce_scatter | solution.py:61
  36.0 1.0 multiply_convert_fusion
  37.0 13.6 %all_gather.6 = bf16[16,6144]{1,0:T(8,128)(2,1)S(1)} all-gather(bf16[16,1536]{1,0:T(8,128)(2,1)S(1)} %multiply_convert_fusion), channel_id=1, replica_groups=mesh['dp'=4,'kv'=4,'tp'=2] {'kv'}, dimensions={1}, use_global_device_ids=true | all-gather | bytes 245760 | tf_op jit(solution)/shard_map/all_gather | solution.py:63
  50.6 0.9 reshape.356
  51.4 0.9 fusion.80
  52.4 0.2 fusion.45
  52.6 0.5 fusion.32
  53.1 0.3 fusion.31
  53.4 13.2 %all-gather.1 = f32[4,12,16]{2,1,0:T(8,128)S(1)} all-gather(f32[1,12,16]{2,1,0:T(8,128)S(1)} %bitcast.103), channel_id=2, replica_groups=mesh['dp'=4,'kv'=4,'tp'=2] {'kv'}, dimensions={0}, use_global_device_ids=true | all-gather | bytes 3840 | tf_op jit(solution)/shard_map/all_gather | solution.py:91
  66.8 0.9 fusion.13
  67.7 0.5 copy-done.2
  68.2 1.0 fusion.14
  69.2 1.8 %bitcast_select_fusion.1 = bf16[1,512,12,128]{3,1,2,0:T(8,128)(2,1)} fusion(bf16[1,512,12,128]{3,1,2,0:T(8,128)(2,1)S(1)} %copy-done.1, pred[512]{0:T(512)(128)(4,1)S(1)} %compare_and_fusion, bf16[1,16,1,12,128]{4,3,2,1,0:T(8,128)(2,1)S(1)} %get-tuple-element.4, s32[512]{0:T(512)S(1)} %fusion.73), kind=kOutput, calls=%fused_computation.3 | convolution fusion | flops 26746880 | bytes 3197440 | tf_op jit(solution)/shard_map/scp,sphd->schd/dot_general | solution.py:118
  70.9 1.8 %bitcast_select_fusion = bf16[1,512,12,128]{3,1,2,0:T(8,128)(2,1)} fusion(bf16[1,512,12,128]{3,1,2,0:T(8,128)(2,1)S(1)} %copy-done.3, pred[512]{0:T(512)(128)(4,1)S(1)} %compare_and_fusion, bf16[1,16,1,12,128]{4,3,2,1,0:T(8,128)(2,1)S(1)} %get-tuple-element.3, s32[512]{0:T(512)S(1)} %fusion.73), kind=kOutput, calls=%fused_computation.2 | convolution fusion | flops 26746880 | bytes 3197440 | tf_op jit(solution)/shard_map/scp,sphd->schd/dot_general | solution.py:121
  72.7 0.3 fusion.21
  73.0 29.2 %all-reduce.2.cloned.1.call-done = f32[1,16,12,128]{3,1,2,0:T(8,128)} async-done(((f32[1,16,12,128]{3,1,2,0:T(8,128)}), f32[1,16,12,128]{3,1,2,0:T(8,128)}) %all-reduce.2.cloned.1.call-update) | async-done | bytes 98320 | tf_op jit(solution)/shard_map/psum | solution.py:105
  102.2 1.1 fusion.17
  103.3 0.3 convolution_convert_fusion.2
  103.6 4.0 %psum.23 = bf16[1,16,512]{2,1,0:T(8,128)(2,1)} all-reduce(bf16[1,16,512]{2,1,0:T(8,128)(2,1)S(1)} %bitcast.102), channel_id=1, replica_groups=mesh['dp'=4,'kv'=4,'tp'=2] {'tp'}, use_global_device_ids=true, to_apply=%region_7.8 | all-reduce | flops 8192 | bytes 32768 | tf_op jit(solution)/shard_map/psum | solution.py:112
  (40 shorter events, 0.7 us)
Async XLA Ops:
  7.2 1.4 %copy-start = (bf16[512,1536]{1,0:T(8,128)(2,1)S(1)}, bf16[512,1536]{1,0:T(8,128)(2,1)}, u32[]{:S(2)}) copy-start(bf16[512,1536]{1,0:T(8,128)(2,1)} %param.15) | copy-start | bytes 4718596
  7.2 2.5 %copy-start.8 = (bf16[1,16,512]{2,1,0:T(8,128)(2,1)S(1)}, bf16[1,16,512]{2,1,0:T(8,128)(2,1)}, u32[]{:S(2)}) copy-start(bf16[1,16,512]{2,1,0:T(8,128)(2,1)} %param.13) | copy-start | bytes 49156
  7.2 2.5 %copy-start.11 = (f32[512]{0:T(512)S(1)}, f32[512]{0:T(512)}, u32[]{:S(2)}) copy-start(f32[512]{0:T(512)} %param.14) | copy-start | bytes 6148
  7.2 2.5 %copy-start.4 = (bf16[512,1536]{1,0:T(8,128)(2,1)S(1)}, bf16[512,1536]{1,0:T(8,128)(2,1)}, u32[]{:S(2)}) copy-start(bf16[512,1536]{1,0:T(8,128)(2,1)} %param.16) | copy-start | bytes 4718596
  7.2 28.8 %reduce-scatter.2.cloned.1.call-start = ((), (), s32[]{:S(2)}) async-start(), calls=%async_computation.1 | async-start | bytes 491520 | tf_op jit(solution)/shard_map/reduce_scatter | solution.py:61
  8.6 1.6 %copy-start.5 = (bf16[512,1536]{1,0:T(8,128)(2,1)S(1)}, bf16[512,1536]{1,0:T(8,128)(2,1)}, u32[]{:S(2)}) copy-start(bf16[512,1536]{1,0:T(8,128)(2,1)} %param.17) | copy-start | bytes 4718596
  9.8 1.5 %copy-start.6 = (bf16[512,1536]{1,0:T(8,128)(2,1)S(1)}, bf16[512,1536]{1,0:T(8,128)(2,1)}, u32[]{:S(2)}) copy-start(bf16[512,1536]{1,0:T(8,128)(2,1)} %param.18) | copy-start | bytes 4718596
  11.3 1.2 %copy-start.13 = (s32[1,16]{1,0:T(1,128)S(1)}, s32[1,16]{1,0:T(1,128)}, u32[]{:S(2)}) copy-start(s32[1,16]{1,0:T(1,128)} %param.25) | copy-start | bytes 196
  11.6 40.8 %copy-start.12 = (f32[12]{0:T(128)S(1)}, f32[12]{0:T(128)}, u32[]{:S(2)}) copy-start(f32[12]{0:T(128)} %param.20) | copy-start | bytes 148
  11.6 41.0 %copy-start.1 = (bf16[1,512,12,128]{3,1,2,0:T(8,128)(2,1)S(1)}, bf16[1,512,12,128]{3,1,2,0:T(8,128)(2,1)}, u32[]{:S(2)}) copy-start(bf16[1,512,12,128]{3,1,2,0:T(8,128)(2,1)} %param.21) | copy-start | bytes 4718596
  12.4 89.8 %all-reduce.2.cloned.1.call-start = ((), (), s32[]{:S(2)}) async-start(), calls=%async_computation.2 | async-start | bytes 196608 | tf_op jit(solution)/shard_map/psum | solution.py:105
  52.5 15.1 %copy-start.9 = (f32[12,16,16]{1,2,0:T(8,128)}, f32[12,16,16]{1,2,0:T(8,128)S(1)}, u32[]{:S(2)}) copy-start(f32[12,16,16]{1,2,0:T(8,128)S(1)} %get-tuple-element.9) | copy-start | bytes 36868
  66.7 1.4 %copy-start.2 = (bf16[1,512,12,128]{3,1,2,0:T(8,128)(2,1)S(1)}, bf16[1,512,12,128]{3,1,2,0:T(8,128)(2,1)}, u32[]{:S(2)}) copy-start(bf16[1,512,12,128]{3,1,2,0:T(8,128)(2,1)} %param.22) | copy-start | bytes 4718596
  69.1 1.8 %copy-start.3 = (bf16[1,512,12,128]{3,1,2,0:T(8,128)(2,1)S(1)}, bf16[1,512,12,128]{3,1,2,0:T(8,128)(2,1)}, u32[]{:S(2)}) copy-start(bf16[1,512,12,128]{3,1,2,0:T(8,128)(2,1)} %param.22) | copy-start | bytes 4718596
  70.9 1.8 %copy-start.10 = (f32[12,16,16]{1,2,0:T(8,128)S(1)}, f32[12,16,16]{1,2,0:T(8,128)}, u32[]{:S(2)}) copy-start(f32[12,16,16]{1,2,0:T(8,128)} %copy-done.9) | copy-start | bytes 36868
  70.9 32.4 %copy-start.7 = (bf16[1536,512]{1,0:T(8,128)(2,1)S(1)}, bf16[1536,512]{1,0:T(8,128)(2,1)}, u32[]{:S(2)}) copy-start(bf16[1536,512]{1,0:T(8,128)(2,1)} %param.19) | copy-start | bytes 4718596
Sparse Core Ops, SparseCore 0:
  12.5 23.4 reduce-scatter.1
  69.3 32.8 all-reduce.1
where the time goes:
time: 115 us; the launch traced here: 114 us
  blocking collectives  44.4 us (39%)
  waiting for transfers between devices  36.8 us (32%)
  between operations  15.6 us (14%)
  matrix products  10.6 us (9%)
  local copies, waits for them, and re-layouts  4.63 us (4%)
  other arithmetic  2.38 us (2%)
    psum x1, waiting for transfers between devices, local(): attended = lax.psum(local_sum, 'kv')  29.2 us
    psum x1, blocking collectives, local(): squares = lax.psum(square_part, 'kv')  13.6 us
    all_gather x1, blocking collectives, local(): lax.all_gather((share * rscale[:, None]).astype(jnp.bfloat16), 'kv', axis...  13.6 us
    all_gather x1, blocking collectives, local(): every = lax.all_gather(shard_rest[None], 'kv', axis=0, tiled=True)  13.2 us
    reduce_scatter x1, waiting for transfers between devices, local(): lax.psum_scatter(partial_value, 'kv', scatter_dimension=1, tiled=True)  7.6 us
    psum x1, blocking collectives, local(): lax.psum(part_out.astype(jnp.bfloat16), 'tp')  3.96 us
    unnamed x28, local copies, waits for them, and re-layouts  2.74 us
  transfers between devices with their start and end apart: 2, of which 2 were waited for; matrix products, arithmetic and copies ran while one was open for 4% of the time, Pallas kernels for 0%

commit v1 on v0

--- a/solution.py
+++ b/solution.py
@@ -60,9 +60,9 @@
     squares = lax.psum(square_part, "kv")
     share = lax.psum_scatter(partial_value, "kv", scatter_dimension=1, tiled=True)
     rscale = lax.rsqrt(squares / D + EPS)
-    projected = lax.all_gather(
-        (share * rscale[:, None]).astype(jnp.bfloat16), "kv", axis=1, tiled=True
-    )
+    own = (share * rscale[:, None]).astype(jnp.bfloat16)
+    shards = lax.all_gather(own, "kv")
+    projected = jnp.concatenate(shards, axis=1)
     shaped = projected.reshape(seqs, props, 4, heads, HEAD)
     query = shaped[:, :, 0]
     key_new = shaped[:, :, 1]

time: 115 us -> 116 us (level)
    unnamed x28 -> x29, local copies, waits for them, and re-layouts: 2.74 us -> 3.44 us
  transfers between devices with their start and end apart: 2 -> 2, of which waited for: 2 -> 2; matrix products, arithmetic and copies ran while one was open for 4% -> 5% of each run, Pallas kernels for 0% -> 0%
where the time goes in v1:
time: 116 us; the launch traced here: 115 us
  blocking collectives  44.4 us (38%)
  waiting for transfers between devices  36.1 us (31%)
  between operations  15.6 us (13%)
  matrix products  11.4 us (10%)
  local copies, waits for them, and re-layouts  5.47 us (5%)
  other arithmetic  2.38 us (2%)
    psum x1, waiting for transfers between devices, local(): attended = lax.psum(local_sum, 'kv')  28.5 us
    psum x1, blocking collectives, local(): squares = lax.psum(square_part, 'kv')  13.6 us
    all_gather x1, blocking collectives, local(): shards = lax.all_gather(own, 'kv')  13.6 us
    all_gather x1, blocking collectives, local(): every = lax.all_gather(shard_rest[None], 'kv', axis=0, tiled=True)  13.2 us
    reduce_scatter x1, waiting for transfers between devices, local(): lax.psum_scatter(partial_value, 'kv', scatter_dimension=1, tiled=True)  7.6 us
    psum x1, blocking collectives, local(): lax.psum(part_out.astype(jnp.bfloat16), 'tp')  3.96 us
    unnamed x29, local copies, waits for them, and re-layouts  3.44 us
  transfers between devices with their start and end apart: 2, of which 2 were waited for; matrix products, arithmetic and copies ran while one was open for 5% of the time, Pallas kernels for 0%

profile of v1, /device:TPU:0, one launch (start us, length us, event | category | flops | bytes accessed | tf_op | source)
XLA Modules:
  0.0 115.4 jit_solution(5456594110192393012)
XLA Ops:
  7.3 1.3 %copy-done = bf16[512,1536]{1,0:T(8,128)(2,1)S(1)} copy-done((bf16[512,1536]{1,0:T(8,128)(2,1)S(1)}, bf16[512,1536]{1,0:T(8,128)(2,1)}, u32[]{:S(2)}) %copy-start) | copy-done | bytes 1572888
  8.6 1.1 fusion.70
  9.8 0.3 fusion.68
  10.1 0.3 fusion.66
  10.4 0.8 copy-done.6
  11.3 0.3 fusion.64
  11.6 0.8 pad_maximum_fusion
  12.4 0.2 fusion.26
  12.9 0.1 fusion.24
  13.0 0.2 fusion.27
  14.7 13.6 %psum.21 = f32[16]{0:T(128)S(1)} all-reduce(f32[16]{0:T(128)S(1)} %fusion.52), channel_id=1, replica_groups=mesh['dp'=4,'kv'=4,'tp'=2] {'kv'}, use_global_device_ids=true, to_apply=%region_2.0 | all-reduce | flops 16 | bytes 128 | tf_op jit(solution)/shard_map/psum | solution.py:60
  28.4 7.6 %reduce-scatter.2.cloned.1.call-done = f32[16,1536]{1,0:T(8,128)} async-done(((f32[16,6144]{1,0:T(8,128)}), f32[16,1536]{1,0:T(8,128)}) %reduce-scatter.2.cloned.1.call-update) | async-done | bytes 98320 | tf_op jit(solution)/shard_map/reduce_scatter | solution.py:61
  36.0 1.0 multiply_convert_fusion
  37.0 13.6 %all-gather = bf16[64,1536]{1,0:T(8,128)(2,1)S(1)} all-gather(bf16[16,1536]{1,0:T(8,128)(2,1)S(1)} %multiply_convert_fusion), channel_id=2, replica_groups=mesh['dp'=4,'kv'=4,'tp'=2] {'kv'}, dimensions={0}, use_global_device_ids=true | all-gather | bytes 245760 | tf_op jit(solution)/shard_map/all_gather | solution.py:64
  50.6 0.2 copy.67
  50.7 0.8 reshape.378
  51.6 0.9 fusion.80
  52.5 0.2 fusion.45
  52.7 0.5 fusion.32
  53.2 0.3 fusion.31
  53.5 13.2 %all-gather.2 = f32[4,12,16]{2,1,0:T(8,128)S(1)} all-gather(f32[1,12,16]{2,1,0:T(8,128)S(1)} %bitcast.112), channel_id=3, replica_groups=mesh['dp'=4,'kv'=4,'tp'=2] {'kv'}, dimensions={0}, use_global_device_ids=true | all-gather | bytes 3840 | tf_op jit(solution)/shard_map/all_gather | solution.py:91
  66.9 0.9 fusion.13
  67.8 0.5 copy-done.2
  68.3 1.0 fusion.14
  69.3 1.8 %bitcast_select_fusion.1 = bf16[1,512,12,128]{3,1,2,0:T(8,128)(2,1)} fusion(bf16[1,512,12,128]{3,1,2,0:T(8,128)(2,1)S(1)} %copy-done.1, pred[512]{0:T(512)(128)(4,1)S(1)} %compare_and_fusion, bf16[1,16,1,12,128]{4,3,2,1,0:T(8,128)(2,1)S(1)} %get-tuple-element.4, s32[512]{0:T(512)S(1)} %fusion.73), kind=kOutput, calls=%fused_computation.3 | convolution fusion | flops 26746880 | bytes 3197440 | tf_op jit(solution)/shard_map/scp,sphd->schd/dot_general | solution.py:118
  71.1 1.8 %bitcast_select_fusion = bf16[1,512,12,128]{3,1,2,0:T(8,128)(2,1)} fusion(bf16[1,512,12,128]{3,1,2,0:T(8,128)(2,1)S(1)} %copy-done.3, pred[512]{0:T(512)(128)(4,1)S(1)} %compare_and_fusion, bf16[1,16,1,12,128]{4,3,2,1,0:T(8,128)(2,1)S(1)} %get-tuple-element.3, s32[512]{0:T(512)S(1)} %fusion.73), kind=kOutput, calls=%fused_computation.2 | convolution fusion | flops 26746880 | bytes 3197440 | tf_op jit(solution)/shard_map/scp,sphd->schd/dot_general | solution.py:121
  72.9 0.3 fusion.21
  73.1 0.7 copy.45
  73.8 28.5 %all-reduce.2.cloned.1.call-done = f32[1,16,12,128]{3,1,2,0:T(8,128)} async-done(((f32[1,16,12,128]{3,1,2,0:T(8,128)}), f32[1,16,12,128]{3,1,2,0:T(8,128)}) %all-reduce.2.cloned.1.call-update) | async-done | bytes 98320 | tf_op jit(solution)/shard_map/psum | solution.py:105
  102.3 1.1 fusion.17
  103.5 1.1 convolution_convert_fusion.2
  104.6 4.0 %psum.23 = bf16[1,16,512]{2,1,0:T(8,128)(2,1)} all-reduce(bf16[1,16,512]{2,1,0:T(8,128)(2,1)S(1)} %bitcast.111), channel_id=1, replica_groups=mesh['dp'=4,'kv'=4,'tp'=2] {'tp'}, use_global_device_ids=true, to_apply=%region_7.8 | all-reduce | flops 8192 | bytes 32768 | tf_op jit(solution)/shard_map/psum | solution.py:112
  (42 shorter events, 1.0 us)
Async XLA Ops:
  7.2 1.4 %copy-start = (bf16[512,1536]{1,0:T(8,128)(2,1)S(1)}, bf16[512,1536]{1,0:T(8,128)(2,1)}, u32[]{:S(2)}) copy-start(bf16[512,1536]{1,0:T(8,128)(2,1)} %param.15) | copy-start | bytes 4718596
  7.2 2.5 %copy-start.8 = (bf16[1,16,512]{2,1,0:T(8,128)(2,1)S(1)}, bf16[1,16,512]{2,1,0:T(8,128)(2,1)}, u32[]{:S(2)}) copy-start(bf16[1,16,512]{2,1,0:T(8,128)(2,1)} %param.13) | copy-start | bytes 49156
  7.2 2.5 %copy-start.11 = (f32[512]{0:T(512)S(1)}, f32[512]{0:T(512)}, u32[]{:S(2)}) copy-start(f32[512]{0:T(512)} %param.14) | copy-start | bytes 6148
  7.2 2.5 %copy-start.4 = (bf16[512,1536]{1,0:T(8,128)(2,1)S(1)}, bf16[512,1536]{1,0:T(8,128)(2,1)}, u32[]{:S(2)}) copy-start(bf16[512,1536]{1,0:T(8,128)(2,1)} %param.16) | copy-start | bytes 4718596
  7.2 28.8 %reduce-scatter.2.cloned.1.call-start = ((), (), s32[]{:S(2)}) async-start(), calls=%async_computation.1 | async-start | bytes 491520 | tf_op jit(solution)/shard_map/reduce_scatter | solution.py:61
  8.6 1.6 %copy-start.5 = (bf16[512,1536]{1,0:T(8,128)(2,1)S(1)}, bf16[512,1536]{1,0:T(8,128)(2,1)}, u32[]{:S(2)}) copy-start(bf16[512,1536]{1,0:T(8,128)(2,1)} %param.17) | copy-start | bytes 4718596
  9.8 1.5 %copy-start.6 = (bf16[512,1536]{1,0:T(8,128)(2,1)S(1)}, bf16[512,1536]{1,0:T(8,128)(2,1)}, u32[]{:S(2)}) copy-start(bf16[512,1536]{1,0:T(8,128)(2,1)} %param.18) | copy-start | bytes 4718596
  11.3 1.2 %copy-start.13 = (s32[1,16]{1,0:T(1,128)S(1)}, s32[1,16]{1,0:T(1,128)}, u32[]{:S(2)}) copy-start(s32[1,16]{1,0:T(1,128)} %param.25) | copy-start | bytes 196
  11.6 40.9 %copy-start.12 = (f32[12]{0:T(128)S(1)}, f32[12]{0:T(128)}, u32[]{:S(2)}) copy-start(f32[12]{0:T(128)} %param.20) | copy-start | bytes 148
  11.6 41.1 %copy-start.1 = (bf16[1,512,12,128]{3,1,2,0:T(8,128)(2,1)S(1)}, bf16[1,512,12,128]{3,1,2,0:T(8,128)(2,1)}, u32[]{:S(2)}) copy-start(bf16[1,512,12,128]{3,1,2,0:T(8,128)(2,1)} %param.21) | copy-start | bytes 4718596
  12.4 90.0 %all-reduce.2.cloned.1.call-start = ((), (), s32[]{:S(2)}) async-start(), calls=%async_computation.2 | async-start | bytes 196608 | tf_op jit(solution)/shard_map/psum | solution.py:105
  52.7 15.1 %copy-start.9 = (f32[12,16,16]{1,2,0:T(8,128)}, f32[12,16,16]{1,2,0:T(8,128)S(1)}, u32[]{:S(2)}) copy-start(f32[12,16,16]{1,2,0:T(8,128)S(1)} %get-tuple-element.11) | copy-start | bytes 36868
  66.9 1.4 %copy-start.2 = (bf16[1,512,12,128]{3,1,2,0:T(8,128)(2,1)S(1)}, bf16[1,512,12,128]{3,1,2,0:T(8,128)(2,1)}, u32[]{:S(2)}) copy-start(bf16[1,512,12,128]{3,1,2,0:T(8,128)(2,1)} %param.22) | copy-start | bytes 4718596
  69.3 1.8 %copy-start.3 = (bf16[1,512,12,128]{3,1,2,0:T(8,128)(2,1)S(1)}, bf16[1,512,12,128]{3,1,2,0:T(8,128)(2,1)}, u32[]{:S(2)}) copy-start(bf16[1,512,12,128]{3,1,2,0:T(8,128)(2,1)} %param.22) | copy-start | bytes 4718596
  71.1 1.8 %copy-start.10 = (f32[12,16,16]{1,2,0:T(8,128)S(1)}, f32[12,16,16]{1,2,0:T(8,128)}, u32[]{:S(2)}) copy-start(f32[12,16,16]{1,2,0:T(8,128)} %copy-done.9) | copy-start | bytes 36868
  72.9 30.6 %copy-start.7 = (bf16[1536,512]{1,0:T(8,128)(2,1)S(1)}, bf16[1536,512]{1,0:T(8,128)(2,1)}, u32[]{:S(2)}) copy-start(bf16[1536,512]{1,0:T(8,128)(2,1)} %param.19) | copy-start | bytes 4718596
Sparse Core Ops, SparseCore 0:
  12.5 23.4 reduce-scatter.1
  69.4 32.8 all-reduce.1
